TPU v7x, 32 devices: a whole 2x2x4 slice. The times are simulated.
32 devices in a mesh: sp: 8 (over z, y), dp: 4 (over x, core).
Axes of the slice: x: 2, y: 2, z: 4, core: 2. Of those that a mesh axis runs over, the one named last changes fastest.
Arguments:
- queries: bfloat16 [16, 16, 512, 128], P('dp', None, 'sp'), may hold values from -6 to 6
- key_maps: bfloat16 [16, 16, 512, 128], P('dp', None, 'sp'), may hold values from -6 to 6
- value_rows: bfloat16 [16, 16, 512, 128], P('dp', None, 'sp'), may hold values from -6 to 6
- gate_logits: bfloat16 [512, 16, 2048], P('sp', 'dp'), may hold values from -6 to 6
- mix_lambda: float32 [16], replicated, may hold values from 0.3 to 0.8
- head_gain: float32 [128], replicated, may hold values from 0.1 to 1.9
- out_weight: bfloat16 [2048, 2048], P('sp', 'dp'), may hold values from -0.125 to 0.125
Outputs:
- projected: bfloat16 [512, 16, 2048], P('sp', 'dp')
All inputs are finite; a program needn't handle non-finite values.
Results may differ from a plain program's by a relative error of at most 0.0075.
Values may be sent and summed in bfloat16 or wider, within the bound.
A program may use at most 64 MiB of HBM per device.

v0:
```python
import functools

import jax
import jax.numpy as jnp
from jax import lax
from jax.experimental import pallas as pl
from jax.experimental.pallas import tpu as pltpu
from jax.sharding import PartitionSpec as P

HEAD_DIM = 64
STRETCH = 64
LOG2E = 1.4426950408889634


def attend_item(q, k, v, weight_two, gain, store):
    length, cols = q.shape
    block = min(2 * STRETCH, length)
    factor = HEAD_DIM ** (-0.5) * LOG2E
    first_map = lax.broadcasted_iota(jnp.int32, (block, cols), 1) < cols // 2
    row_seg = (lax.broadcasted_iota(jnp.int32, (2 * block, block), 0) % block) // STRETCH
    col_seg = lax.broadcasted_iota(jnp.int32, (2 * block, block), 1) // STRETCH
    visible = col_seg <= row_seg
    for lo in range(0, length, block):
        hi = lo + block
        rows = q[lo:hi]
        zero = jnp.zeros_like(rows)
        both = jnp.concatenate([jnp.where(first_map, rows, zero), jnp.where(first_map, zero, rows)], axis=0)
        scores = lax.dot_general(
            both, k[:hi], (((1,), (1,)), ((), ())), preferred_element_type=jnp.float32
        )
        diag = jnp.where(visible, scores[:, lo:], -1e30)
        scores = jnp.concatenate([scores[:, :lo], diag], axis=1) if lo else diag
        highest = jnp.max(scores, axis=1, keepdims=True)
        weights = jnp.exp2((scores - highest) * factor)
        summed = jnp.sum(weights, axis=1, keepdims=True)
        mapped = (
            jnp.dot(weights.astype(jnp.bfloat16), v[:hi], preferred_element_type=jnp.float32) / summed
        )
        combined = mapped[:block] - weight_two * mapped[block:]
        mean_sq = jnp.mean(combined * combined, axis=1, keepdims=True)
        store(lo, (combined * lax.rsqrt(mean_sq + 1e-05) * gain).astype(jnp.bfloat16))


def exchange_kernel(n, heads, q_ref, k_ref, v_ref, lam_ref, gain_ref, ret_ref, recv, staged, send_sem, recv_sem, back_sem, ret_sem):
    me = lax.axis_index("sp")
    items, toks, cols = q_ref.shape
    per_dev = items // n
    length = n * toks

    barrier = pltpu.get_barrier_semaphore()

    def greet(step, carry):
        pl.semaphore_signal(barrier, inc=1, device_id={"sp": lax.rem(me + step, n)})
        return carry

    lax.fori_loop(1, n, greet, 0)
    pl.semaphore_wait(barrier, n - 1)

    def send_item(j, carry):
        for which, ref in enumerate((q_ref, k_ref, v_ref)):
            pltpu.make_async_copy(
                ref.at[me * per_dev + j], recv.at[j, which, me], recv_sem.at[j]
            ).start()

        def to_peer(step, carry):
            peer = lax.rem(me + step, n)
            for which, ref in enumerate((q_ref, k_ref, v_ref)):
                pltpu.make_async_remote_copy(
                    src_ref=ref.at[peer * per_dev + j],
                    dst_ref=recv.at[j, which, me],
                    send_sem=send_sem.at[j],
                    recv_sem=recv_sem.at[j],
                    device_id={"sp": peer},
                ).start()
            return carry

        return lax.fori_loop(1, n, to_peer, carry)

    lax.fori_loop(0, per_dev, send_item, 0)

    gain = gain_ref[...]

    def work_item(j, carry):
        pltpu.make_async_copy(recv.at[j], recv.at[j], recv_sem.at[j]).wait()
        q = recv[j, 0].reshape(length, cols)
        k = recv[j, 1].reshape(length, cols)
        v = recv[j, 2].reshape(length, cols)
        item = me * per_dev + j

        def store(lo, rows):
            for r in range(0, rows.shape[0], toks):
                staged[j, (lo + r) // toks] = rows[r : r + toks]

        attend_item(q, k, v, lam_ref[lax.rem(item, heads)], gain, store)
        pltpu.make_async_copy(staged.at[j, me], ret_ref.at[item], ret_sem).start()

        def to_peer(step, carry):
            peer = lax.rem(me + step, n)
            pltpu.make_async_remote_copy(
                src_ref=staged.at[j, peer],
                dst_ref=ret_ref.at[item],
                send_sem=back_sem,
                recv_sem=ret_sem,
                device_id={"sp": peer},
            ).start()
            return carry

        return lax.fori_loop(1, n, to_peer, carry)

    lax.fori_loop(0, per_dev, work_item, 0)
    pltpu.make_async_copy(ret_ref, ret_ref, ret_sem).wait()
    others = staged.at[:, pl.ds(0, n - 1)]
    pltpu.make_async_copy(others, others, back_sem).wait()

    def drain(j, carry):
        for which in range(3):
            part = recv.at[j, which, pl.ds(0, n - 1)]
            pltpu.make_async_copy(part, part, send_sem.at[j]).wait()
        return carry

    lax.fori_loop(0, per_dev, drain, 0)


def on_device(n, queries, key_maps, value_rows, gate_logits, mix_lambda, head_gain, out_weight):
    seqs, heads, toks, cols = queries.shape
    items = seqs * heads
    per_dev = items // n
    width = gate_logits.shape[2]
    anywhere = pl.BlockSpec(memory_space=pl.ANY)
    in_vmem = pl.BlockSpec(memory_space=pltpu.VMEM)
    returned = pl.pallas_call(
        functools.partial(exchange_kernel, n, heads),
        out_shape=jax.ShapeDtypeStruct((items, toks, cols), jnp.bfloat16),
        in_specs=[anywhere, anywhere, anywhere, pl.BlockSpec(memory_space=pltpu.SMEM), in_vmem],
        out_specs=in_vmem,
        scratch_shapes=[
            pltpu.VMEM((per_dev, 3, n, toks, cols), jnp.bfloat16),
            pltpu.VMEM((per_dev, n, toks, cols), jnp.bfloat16),
            pltpu.SemaphoreType.DMA((per_dev,)),
            pltpu.SemaphoreType.DMA((per_dev,)),
            pltpu.SemaphoreType.DMA,
            pltpu.SemaphoreType.DMA,
        ],
        compiler_params=pltpu.CompilerParams(
            collective_id=0, has_side_effects=True, vmem_limit_bytes=40 * 2**20
        ),
        cost_estimate=pl.CostEstimate(flops=5 * 10**10, bytes_accessed=2**28, transcendentals=0),
    )(
        queries.reshape(items, toks, cols),
        key_maps.reshape(items, toks, cols),
        value_rows.reshape(items, toks, cols),
        mix_lambda,
        head_gain.reshape(1, cols),
    )
    by_token = jnp.transpose(returned.reshape(seqs, heads, toks, cols), (2, 0, 1, 3)).reshape(
        toks, seqs, width
    )
    gated = (jax.nn.sigmoid(gate_logits.astype(jnp.float32)) * by_token.astype(jnp.float32)).astype(
        jnp.bfloat16
    )
    gathered = lax.all_gather(out_weight, ("dp", "sp"), axis=0, tiled=True)
    result = jnp.einsum(
        "tk,ckn->tcn",
        gated.reshape(toks * seqs, width),
        gathered.reshape(-1, width, out_weight.shape[1]),
        preferred_element_type=jnp.float32,
    )
    return result.astype(jnp.bfloat16).reshape(toks, seqs, width)


def solution(mesh):
    placed = (
        P("dp", None, "sp", None),
        P("dp", None, "sp", None),
        P("dp", None, "sp", None),
        P("sp", "dp", None),
        P(),
        P(),
        P("sp", "dp"),
    )
    return jax.shard_map(
        functools.partial(on_device, mesh.shape["sp"]),
        mesh=mesh,
        in_specs=placed,
        out_specs=P("sp", "dp", None),
        check_vma=False,
    )
```

profile of v0, /device:TPU:0, one launch (start us, length us, event | category | flops | bytes accessed | tf_op | source)
XLA Modules:
  0.0 169.6 jit_solution(16107531002783766022)
XLA Ops:
  6.5 0.0 all-gather.2.cloned.1.call-start
  6.5 0.7 all-gather.2.cloned.1.call-update
  7.3 0.0 copy-start
  7.3 1.2 copy-done
  8.5 0.0 copy-start.1
  8.5 1.2 copy-done.1
  9.7 0.0 copy-start.2
  9.7 1.2 copy-done.2
  10.9 0.0 copy-start.3
  10.9 0.7 copy-done.3
  11.6 0.0 copy-start.4
  11.6 0.7 copy-done.4
  12.2 136.3 %shard_map.73 = bf16[64,64,128]{2,1,0:T(8,128)(2,1)S(1)} custom-call(bf16[64,64,128]{2,1,0:T(8,128)(2,1)S(1)} %bitcast.14, bf16[64,64,128]{2,1,0:T(8,128)(2,1)S(1)} %bitcast.15, bf16[64,64,128]{2,1,0:T(8,128)(2,1)S(1)} %bitcast.16, f32[16]{0:T(128)S(1)} %copy-done.3, f32[1,128]{1,0:T(1,128)S(1)} %bitcast.17), custom_call_target="tpu_custom_call" | custom-call | flops 49999998976 | bytes 268435456 | tf_op jit(solution)/shard_map/pallas_call | solution.py:131
  148.5 0.2 convert_bitcast_fusion
  148.8 1.2 copy.9
  150.0 0.0 copy-start.5
  150.0 1.7 %reshape.34 = f32[64,4,2048]{2,1,0:T(4,128)} reshape(f32[64,4,16,128]{3,2,1,0:T(8,128)S(1)} %copy.9) | data formatting | bytes 4194304 | tf_op jit(solution)/shard_map/convert_element_type | solution.py:158
  151.7 0.0 copy-done.5
  151.7 2.7 %fusion = bf16[64,4,2048]{2,1,0:T(4,128)(2,1)S(1)} fusion(f32[64,4,2048]{2,1,0:T(4,128)} %reshape.34, bf16[64,4,2048]{2,1,0:T(4,128)(2,1)S(1)} %copy-done.5), kind=kLoop, calls=%fused_computation.2 | loop fusion | flops 3145728 | bytes 4194304 | tf_op jit(solution)/shard_map/convert_element_type | solution.py:158
  154.4 0.3 reshape.36
  154.7 0.0 all-gather.2.cloned.1.call-done
  154.8 5.7 %convolution_convert_fusion = bf16[256,4,512]{2,0,1:T(8,128)(2,1)S(1)} fusion(bf16[256,2048,1]{1,0,2:T(8,128)(2,1)S(1)} %reshape.36, bf16[4,2048,512]{2,1,0:T(8,128)(2,1)} %bitcast.18), kind=kOutput, calls=%fused_computation.3 | convolution fusion | flops 2148007936 | bytes 10485760 | tf_op jit(solution)/shard_map/tk,ckn->tcn/dot_general | solution.py:162
  160.5 0.8 copy.10
  161.3 1.5 reshape.33
Async XLA Ops:
  6.5 148.2 %all-gather.2.cloned.1.call-start = ((), (), s32[]{:S(2)}) async-start(), calls=%async_computation | async-start | bytes 8650752 | tf_op jit(solution)/shard_map/all_gather | solution.py:161
  7.3 1.2 copy-start
  8.5 1.2 copy-start.1
  9.7 1.2 copy-start.2
  10.9 0.7 copy-start.3
  11.6 0.7 copy-start.4
  150.0 1.8 %copy-start.5 = (bf16[64,4,2048]{2,1,0:T(4,128)(2,1)S(1)}, bf16[64,4,2048]{2,1,0:T(4,128)(2,1)}, u32[]{:S(2)}) copy-start(bf16[64,4,2048]{2,1,0:T(4,128)(2,1)} %param.10) | copy-start | bytes 3145732
Sparse Core Ops, SparseCore 0:
  10.3 118.7 all-gather.1
where the time goes:
time: 170 us
  Pallas kernels  136 us (80%)
  between operations  13.5 us (8%)
  local copies, waits for them, and re-layouts  10.5 us (6%)
  matrix products  5.7 us (3%)
  other arithmetic  2.93 us (2%)
    pallas_call x1, Pallas kernels, on_device(): pl.pallas_call(functools.partial(exchange_kernel, n, heads), out_shape=ja...  136 us
    dot_general x1, matrix products, on_device(): jnp.einsum('tk,ckn->tcn', gated.reshape(toks * seqs, width), gathered.res...  5.7 us
    unnamed x12, local copies, waits for them, and re-layouts  4.98 us
  transfers between devices with their start and end apart: 1, of which 0 were waited for; matrix products, arithmetic and copies ran while one was open for 4% of the time, Pallas kernels for 80%

commit v1 on v0

v1 whole, which is shorter than its diff:
```python
import functools

import jax
import jax.numpy as jnp
from jax import lax
from jax.experimental import pallas as pl
from jax.experimental.pallas import tpu as pltpu
from jax.sharding import PartitionSpec as P

HEAD_DIM = 64
STRETCH = 64
LOG2E = 1.4426950408889634
WINDOW = 8


def plan(n, items):
    rows = items // (n // 4)
    singles = 2 * ((rows * 7) // 32)
    doubles = rows - singles
    outer_single = singles * 2 // 7
    inner_double = doubles // 6
    groups = [
        (outer_single, 0, 0),
        (singles - outer_single, 0, 1),
        (doubles - inner_double, 1, 0),
        (inner_double, 1, 1),
    ]
    order = sorted(
        ((i + 0.5) / count, g) for g, (count, _, _) in enumerate(groups) for i in range(count)
    )
    kinds, lows, highs, seen = [], [], [], 0
    for _, g in order:
        _, kind, low = groups[g]
        kinds.append(kind)
        lows.append(low)
        highs.append(2 + seen % 2)
        seen += kind
    return kinds, lows, highs


def pick(table, index):
    value = jnp.int32(table[0])
    for i, entry in enumerate(table[1:], 1):
        value = jnp.where(index == i, entry, value)
    return value


def attend(q, k, v, start, weight_two, gain, store):
    rows_all, cols = q.shape
    block = min(2 * STRETCH, rows_all)
    factor = HEAD_DIM ** (-0.5) * LOG2E
    first_map = lax.broadcasted_iota(jnp.int32, (block, cols), 1) < cols // 2
    row_seg = (lax.broadcasted_iota(jnp.int32, (2 * block, block), 0) % block) // STRETCH
    col_seg = lax.broadcasted_iota(jnp.int32, (2 * block, block), 1) // STRETCH
    visible = col_seg <= row_seg
    for at in range(0, rows_all, block):
        lo = start + at
        hi = lo + block
        rows = q[at : at + block]
        zero = jnp.zeros_like(rows)
        both = jnp.concatenate([jnp.where(first_map, rows, zero), jnp.where(first_map, zero, rows)], axis=0)
        scores = lax.dot_general(
            both, k[:hi], (((1,), (1,)), ((), ())), preferred_element_type=jnp.float32
        )
        diag = jnp.where(visible, scores[:, lo:], -1e30)
        scores = jnp.concatenate([scores[:, :lo], diag], axis=1) if lo else diag
        highest = jnp.max(scores, axis=1, keepdims=True)
        weights = jnp.exp2((scores - highest) * factor)
        summed = jnp.sum(weights, axis=1, keepdims=True)
        mapped = (
            jnp.dot(weights.astype(jnp.bfloat16), v[:hi], preferred_element_type=jnp.float32) / summed
        )
        combined = mapped[:block] - weight_two * mapped[block:]
        mean_sq = jnp.mean(combined * combined, axis=1, keepdims=True)
        store(at, (combined * lax.rsqrt(mean_sq + 1e-05) * gain).astype(jnp.bfloat16))


def layer_kernel(
    n, m, heads, q_ref, k_ref, v_ref, gate_ref, lam_ref, gain_ref, w_ref, out_ref,
    recv, staged, ret, wbuf, gate_v, gated,
    recv_sem, send_sem, ret_sem, back_sem, w_sem, w_send_sem, gate_sem,
):
    me = lax.axis_index("sp")
    col = lax.axis_index("dp")
    items, toks, cols = q_ref.shape
    seqs = items // heads
    half = n // 2
    quarter = n // 4
    rows = items // quarter
    kinds, lows, highs = plan(n, items)
    low = me < half
    my_quarter = me // quarter
    my_column = lax.rem(me, quarter)
    w_rows, w_cols = w_ref.shape

    cores = 2 if m % 2 == 0 else 1
    xs = m // cores
    ys = 1
    while 2 * (2 * ys) ** 2 <= n:
        ys *= 2
    zs = n // ys
    hz = zs // 2
    my_z, my_y = me // ys, lax.rem(me, ys)
    my_x, my_core = col // cores, lax.rem(col, cores)

    barrier = pltpu.get_barrier_semaphore()

    def greet_sp(step, carry):
        pl.semaphore_signal(barrier, inc=1, device_id={"sp": lax.rem(me + step, n)})
        return carry

    def greet_dp(step, carry):
        pl.semaphore_signal(barrier, inc=1, device_id={"dp": lax.rem(col + step, m)})
        return carry

    gate_copy = pltpu.make_async_copy(gate_ref, gate_v, gate_sem)
    gate_copy.start()
    lax.fori_loop(1, n, greet_sp, 0)
    lax.fori_loop(1, m, greet_dp, 0)

    def w_at(s, d):
        return wbuf.at[d, pl.ds(pl.multiple_of(s * w_rows, w_rows), w_rows)]

    pltpu.make_async_copy(w_ref, w_at(me, col), w_sem.at[me, col]).start()
    pl.semaphore_wait(barrier, n - 1 + m - 1)

    def w_send(src, s, d, **target):
        pltpu.make_async_remote_copy(
            src_ref=src, dst_ref=w_at(s, d), send_sem=w_send_sem, recv_sem=w_sem.at[s, d], device_id=target
        ).start()

    def w_wait(s, d):
        pltpu.make_async_copy(w_at(s, d), w_at(s, d), w_sem.at[s, d]).wait()

    def to_half_peers(src, s, d):
        for i in range(1, hz):
            base = (my_z // hz) * hz
            w_send(src, s, d, sp=(base + lax.rem(my_z - base + i, hz)) * ys + my_y)

    def to_ys(src, s, d):
        for i in range(1, ys):
            w_send(src, s, d, sp=my_z * ys + lax.rem(my_y + i, ys))

    def to_xs(src, s, d):
        for i in range(1, xs):
            w_send(src, s, d, dp=lax.rem(my_x + i, xs) * cores + my_core)

    def to_core(src, s, d):
        if cores > 1:
            w_send(src, s, d, dp=my_x * cores + (1 - my_core))

    base_z = (my_z // hz) * hz
    far_z = hz - base_z
    is_gate = my_z == jnp.where(low, hz - 1, hz)

    w_send(w_ref, me, col, sp=jnp.where(low, hz, hz - 1) * ys + my_y)
    to_half_peers(w_ref, me, col)
    to_ys(w_ref, me, col)
    to_xs(w_ref, me, col)
    to_core(w_ref, me, col)

    def w_near():
        for i in range(1, ys):
            s = my_z * ys + lax.rem(my_y + i, ys)
            w_wait(s, col)
            to_xs(w_at(s, col), s, col)
            to_core(w_at(s, col), s, col)
        for i in range(1, hz):
            s = (base_z + lax.rem(my_z - base_z + i, hz)) * ys + my_y
            w_wait(s, col)
            to_ys(w_at(s, col), s, col)
            to_xs(w_at(s, col), s, col)
            to_core(w_at(s, col), s, col)

    def w_far(gateway):
        for i in range(hz):
            s = (far_z + i) * ys + my_y
            w_wait(s, col)
            if gateway:
                to_half_peers(w_at(s, col), s, col)
            to_ys(w_at(s, col), s, col)
            to_xs(w_at(s, col), s, col)
            to_core(w_at(s, col), s, col)

    def w_side():
        for j in range(1, ys):
            for i in range(1, zs):
                s = lax.rem(my_z + i, zs) * ys + lax.rem(my_y + j, ys)
                w_wait(s, col)
                to_xs(w_at(s, col), s, col)
                to_core(w_at(s, col), s, col)

    def w_across():
        for i in range(1, xs):
            d = lax.rem(my_x + i, xs) * cores + my_core

            def forward(s, carry):
                w_wait(s, d)
                to_core(w_at(s, d), s, d)
                return carry

            lax.fori_loop(0, n, forward, 0)

    def w_last():
        if cores > 1:
            for i in range(xs):
                d = i * cores + (1 - my_core)

                def arrive(s, carry):
                    w_wait(s, d)
                    return carry

                lax.fori_loop(0, n, arrive, 0)
        w_wait(me, col)

    near = 1 + (hz - 1) + (ys - 1) + (xs - 1) + (cores - 1)
    passed = (n - 1) * (xs - 1 + cores - 1) + (zs - 1) * (ys - 1) + n * (xs - 1) * (cores - 1)
    w_sends = near + passed + jnp.where(is_gate, hz * (hz - 1), 0)

    def send_row(r):
        kind, low_q, high_q = pick(kinds, r), pick(lows, r), pick(highs, r)

        def send_item(c, carry):
            item = r * quarter + c
            first = jnp.where((kind == 0) | low, low_q, high_q) * quarter + c

            @pl.when(first == me)
            def _():
                for which, ref in enumerate((q_ref, k_ref, v_ref)):
                    pltpu.make_async_copy(ref.at[item], recv.at[r, which * n + me], recv_sem.at[r]).start()

            def far(which, ref, peer):
                pltpu.make_async_remote_copy(
                    src_ref=ref.at[item],
                    dst_ref=recv.at[r, which * n + me],
                    send_sem=send_sem,
                    recv_sem=recv_sem.at[r],
                    device_id={"sp": peer},
                ).start()

            @pl.when(first != me)
            def _():
                for which, ref in enumerate((q_ref, k_ref, v_ref)):
                    far(which, ref, first)

            @pl.when((kind == 1) & low)
            def _():
                far(1, k_ref, high_q * quarter + c)
                far(2, v_ref, high_q * quarter + c)

            return carry

        lax.fori_loop(0, quarter, send_item, 0)

    def send_first(r, carry):
        send_row(r)
        return carry

    lax.fori_loop(0, min(WINDOW, rows), send_first, 0)
    w_near()

    gain = gain_ref[...]

    def arrived(part, sem):
        pltpu.make_async_copy(part, part, sem).wait()

    def work_row(r, carry):
        @pl.when(r + WINDOW < rows)
        def _():
            send_row(r + WINDOW)

        kind, low_q, high_q = pick(kinds, r), pick(lows, r), pick(highs, r)
        item = r * quarter + my_column
        weight_two = lam_ref[lax.rem(item, heads)]
        is_low = low & (low_q == my_quarter)
        is_high = jnp.logical_not(low) & (kind == 1) & (high_q == my_quarter)

        def part(first, count):
            q = recv[r, first : first + count].reshape(count * toks, cols)
            k = recv[r, n : n + first + count].reshape((first + count) * toks, cols)
            v = recv[r, 2 * n : 2 * n + first + count].reshape((first + count) * toks, cols)

            def store(at, block):
                for i in range(0, block.shape[0], toks):
                    staged[r, first + (at + i) // toks] = block[i : i + toks]

            attend(q, k, v, first * toks, weight_two, gain, store)
            for s in range(first, first + count):

                @pl.when(me == s)
                def _():
                    pltpu.make_async_copy(staged.at[r, s], ret.at[item], ret_sem).start()

                @pl.when(me != s)
                def _():
                    pltpu.make_async_remote_copy(
                        src_ref=staged.at[r, s],
                        dst_ref=ret.at[item],
                        send_sem=back_sem,
                        recv_sem=ret_sem,
                        device_id={"sp": s},
                    ).start()

        @pl.when(is_low & (kind == 0))
        def _():
            arrived(recv.at[r], recv_sem.at[r])

        @pl.when(is_low & (kind == 1))
        def _():
            arrived(recv.at[r, pl.ds(0, 3 * half)], recv_sem.at[r])

        @pl.when(is_high)
        def _():
            arrived(recv.at[r, pl.ds(half, 3 * n - half)], recv_sem.at[r])

        @pl.when(is_low)
        def _():
            part(0, half)

        @pl.when((is_low & (kind == 0)) | is_high)
        def _():
            part(half, half)

        @pl.when((r == rows // 16) & is_gate)
        def _():
            w_far(True)

        @pl.when((r == rows // 4) & jnp.logical_not(is_gate))
        def _():
            w_far(False)

        @pl.when(r == rows // 2)
        def _():
            w_side()

        @pl.when(r == rows - rows // 4)
        def _():
            w_across()

        return carry

    lax.fori_loop(0, rows, work_row, 0)
    w_last()

    n_single = [sum(1 for k, l in zip(kinds, lows) if k == 0 and l == i) for i in range(2)]
    n_double = [sum(1 for k, l in zip(kinds, lows) if k == 1 and l == i) for i in range(2)]
    n_high = [sum(1 for k, h in zip(kinds, highs) if k == 1 and h == i) for i in (2, 3)]
    doubles = sum(kinds) * quarter
    mine = [n_single[i] + n_double[i] for i in range(2)] + n_high
    sent = items - pick(mine, my_quarter)
    backs = pick(
        [mine[i] * (half - 1) + n_single[i] * half for i in range(2)] + [h * (half - 1) for h in n_high],
        my_quarter,
    )

    def drain(part, sem, count):
        def one(i, carry):
            pltpu.make_async_copy(part, part, sem).wait()
            return carry

        lax.fori_loop(0, count, one, 0)

    drain(recv.at[0, pl.ds(0, 3)], send_sem, sent)
    drain(recv.at[0, pl.ds(0, 2)], send_sem, jnp.where(low, doubles, 0))
    drain(w_at(me, col), w_send_sem, w_sends)

    gate_copy.wait()
    pltpu.make_async_copy(ret, ret, ret_sem).wait()
    for s in range(seqs):
        for h in range(heads):
            logits = gate_v[:, s, h * cols : (h + 1) * cols].astype(jnp.float32)
            gated[s * toks : (s + 1) * toks, h * cols : (h + 1) * cols] = (
                jax.nn.sigmoid(logits) * ret[s * heads + h].astype(jnp.float32)
            ).astype(jnp.bfloat16)
    for d in range(m):
        result = jnp.dot(gated[...], wbuf[d], preferred_element_type=jnp.float32)
        for s in range(seqs):
            out_ref[s, :, d * w_cols : (d + 1) * w_cols] = result[s * toks : (s + 1) * toks].astype(
                jnp.bfloat16
            )
    drain(staged.at[0, 0], back_sem, backs)


def on_device(n, m, queries, key_maps, value_rows, gate_logits, mix_lambda, head_gain, out_weight):
    seqs, heads, toks, cols = queries.shape
    items = seqs * heads
    rows = items // (n // 4)
    width = gate_logits.shape[2]
    w_rows, w_cols = out_weight.shape
    anywhere = pl.BlockSpec(memory_space=pl.ANY)
    in_vmem = pl.BlockSpec(memory_space=pltpu.VMEM)
    result = pl.pallas_call(
        functools.partial(layer_kernel, n, m, heads),
        out_shape=jax.ShapeDtypeStruct((seqs, toks, width), jnp.bfloat16),
        in_specs=[
            anywhere, anywhere, anywhere, anywhere, pl.BlockSpec(memory_space=pltpu.SMEM), in_vmem, anywhere,
        ],
        out_specs=in_vmem,
        scratch_shapes=[
            pltpu.VMEM((rows, 3 * n, toks, cols), jnp.bfloat16),
            pltpu.VMEM((rows, n, toks, cols), jnp.bfloat16),
            pltpu.VMEM((items, toks, cols), jnp.bfloat16),
            pltpu.VMEM((m, n * w_rows, w_cols), jnp.bfloat16),
            pltpu.VMEM(gate_logits.shape, jnp.bfloat16),
            pltpu.VMEM((seqs * toks, width), jnp.bfloat16),
            pltpu.SemaphoreType.DMA((rows,)),
            pltpu.SemaphoreType.DMA,
            pltpu.SemaphoreType.DMA,
            pltpu.SemaphoreType.DMA,
            pltpu.SemaphoreType.DMA((n, m)),
            pltpu.SemaphoreType.DMA,
            pltpu.SemaphoreType.DMA,
        ],
        compiler_params=pltpu.CompilerParams(
            collective_id=0, has_side_effects=True, vmem_limit_bytes=60 * 2**20
        ),
        cost_estimate=pl.CostEstimate(flops=5 * 10**10, bytes_accessed=2**28, transcendentals=0),
    )(
        queries.reshape(items, toks, cols),
        key_maps.reshape(items, toks, cols),
        value_rows.reshape(items, toks, cols),
        gate_logits,
        mix_lambda,
        head_gain.reshape(1, cols),
        out_weight,
    )
    return jnp.transpose(result, (1, 0, 2))


def solution(mesh):
    placed = (
        P("dp", None, "sp", None),
        P("dp", None, "sp", None),
        P("dp", None, "sp", None),
        P("sp", "dp", None),
        P(),
        P(),
        P("sp", "dp"),
    )
    return jax.shard_map(
        functools.partial(on_device, mesh.shape["sp"], mesh.shape["dp"]),
        mesh=mesh,
        in_specs=placed,
        out_specs=P("sp", "dp", None),
        check_vma=False,
    )
```

time: 170 us -> 117 us (0.69)
  Pallas kernels: 136 us -> 114 us
  between operations: 13.5 us -> 0.01 us
  local copies, waits for them, and re-layouts: 10.5 us -> 3.01 us
  matrix products: 5.7 us -> 0 us
  other arithmetic: 2.93 us -> 0 us
    pallas_call x1, Pallas kernels: 136 us -> 114 us  [on_device(): pl.pallas_call(functools.partial(layer_kernel, n, m, heads), out_shape=ja...]
    dot_general x1 -> x0, matrix products: 5.7 us -> none  [on_device(): jnp.einsum('tk,ckn->tcn', gated.reshape(toks * seqs, width), gathered.res...]
    unnamed x12 -> x0, local copies, waits for them, and re-layouts: 4.98 us -> none
    convert_element_type x3 -> x0, local copies, waits for them, and re-layouts: 3.78 us -> none  [the longest x2 2.97 us: on_device(): by_token.astype(jnp.float32)]
    transpose x0 -> x1, local copies, waits for them, and re-layouts: none -> 3.01 us  [on_device(): return jnp.transpose(result, (1, 0, 2))]
    convert_element_type x2 -> x0, other arithmetic: 2.93 us -> none  [the longest x1 2.68 us: on_device(): (jax.nn.sigmoid(gate_logits.astype(jnp.float32)) * by_token.astype(jnp.fl...]
    reshape x2 -> x0, local copies, waits for them, and re-layouts: 1.77 us -> none  [the longest x1 1.49 us: on_device(): return result.astype(jnp.bfloat16).reshape(toks, seqs, width)]
  transfers between devices with their start and end apart: 1 -> 0, of which waited for: 0 -> 0; matrix products, arithmetic and copies ran while one was open for 4% -> 0% of each run, Pallas kernels for 80% -> 0%
where the time goes in v1:
time: 117 us
  Pallas kernels  114 us (97%)
  local copies, waits for them, and re-layouts  3.01 us (3%)
    pallas_call x1, Pallas kernels, on_device(): pl.pallas_call(functools.partial(layer_kernel, n, m, heads), out_shape=ja...  114 us
    transpose x1, local copies, waits for them, and re-layouts, on_device(): return jnp.transpose(result, (1, 0, 2))  3.01 us

profile of v1, /device:TPU:0, one launch (start us, length us, event | category | flops | bytes accessed | tf_op | source)
XLA Modules:
  0.0 117.0 jit_solution(5364675971428107711)
XLA Ops:
  0.0 114.0 %shard_map.73 = bf16[4,64,2048]{2,1,0:T(8,128)(2,1)} custom-call(bf16[64,64,128]{2,1,0:T(8,128)(2,1)} %bitcast.6, bf16[64,64,128]{2,1,0:T(8,128)(2,1)} %bitcast.7, bf16[64,64,128]{2,1,0:T(8,128)(2,1)} %bitcast.8, bf16[64,4,2048]{2,1,0:T(4,128)(2,1)} %gate_ref.1, f32[16]{0:T(128)} %lam_ref.1, f32[1,128]{1,0:T(1,128)} %bitcast.9, bf16[256,512]{1,0:T(8,128)(2,1)} %w_ref.1), custom_call_target="tpu_custom_call" | custom-call | flops 49999998976 | bytes 268435456 | tf_op jit(solution)/shard_map/pallas_call | solution.py:392
  114.0 3.0 %copy.8 = bf16[64,4,2048]{2,1,0:T(4,128)(2,1)} copy(bf16[64,4,2048]{2,0,1:T(8,128)(2,1)} %bitcast.5) | data formatting | bytes 2097152 | tf_op jit(solution)/shard_map/transpose | solution.py:427

commit v2 on v1

--- a/solution.py
+++ b/solution.py
@@ -10,7 +10,13 @@
 HEAD_DIM = 64
 STRETCH = 64
 LOG2E = 1.4426950408889634
-WINDOW = 8
+GROUPS = 8
+WINDOW = 16
+NEAR = 0
+GATE = 1
+FAR = 9
+SIDE = 17
+ACROSS = 25
 
 
 def plan(n, items):
@@ -36,6 +42,10 @@
         highs.append(2 + seen % 2)
         seen += kind
     return kinds, lows, highs
+
+
+def item_at(place, seqs, heads):
+    return lax.rem(place, seqs) * heads + place // seqs
 
 
 def pick(table, index):
@@ -77,7 +87,7 @@
 
 def layer_kernel(
     n, m, heads, q_ref, k_ref, v_ref, gate_ref, lam_ref, gain_ref, w_ref, out_ref,
-    recv, staged, ret, wbuf, gate_v, gated,
+    recv, staged, ret, wbuf, gate_v, gated, partial,
     recv_sem, send_sem, ret_sem, back_sem, w_sem, w_send_sem, gate_sem,
 ):
     me = lax.axis_index("sp")
@@ -221,7 +231,7 @@
         kind, low_q, high_q = pick(kinds, r), pick(lows, r), pick(highs, r)
 
         def send_item(c, carry):
-            item = r * quarter + c
+            item = item_at(r * quarter + c, seqs, heads)
             first = jnp.where((kind == 0) | low, low_q, high_q) * quarter + c
 
             @pl.when(first == me)
@@ -257,7 +267,11 @@
         return carry
 
     lax.fori_loop(0, min(WINDOW, rows), send_first, 0)
-    w_near()
+
+    gate_copy.wait()
+    for h in range(heads):
+        logits = gate_v[:, :, h * cols : (h + 1) * cols].astype(jnp.float32)
+        gated[h] = jax.nn.sigmoid(logits).reshape(toks * seqs, cols)
 
     gain = gain_ref[...]
 
@@ -269,9 +283,31 @@
         def _():
             send_row(r + WINDOW)
 
+        @pl.when(r == NEAR * rows // 32)
+        def _():
+            w_near()
+
+        @pl.when((r == GATE * rows // 32) & is_gate)
+        def _():
+            w_far(True)
+
+        @pl.when((r == FAR * rows // 32) & jnp.logical_not(is_gate))
+        def _():
+            w_far(False)
+
+        @pl.when(r == SIDE * rows // 32)
+        def _():
+            w_side()
+
+        @pl.when(r == ACROSS * rows // 32)
+        def _():
+            w_across()
+
         kind, low_q, high_q = pick(kinds, r), pick(lows, r), pick(highs, r)
-        item = r * quarter + my_column
-        weight_two = lam_ref[lax.rem(item, heads)]
+        place = r * quarter + my_column
+        item = item_at(place, seqs, heads)
+        group = place // (items // GROUPS)
+        weight_two = lam_ref[place // seqs]
         is_low = low & (low_q == my_quarter)
         is_high = jnp.logical_not(low) & (kind == 1) & (high_q == my_quarter)
 
@@ -289,15 +325,15 @@
 
                 @pl.when(me == s)
                 def _():
-                    pltpu.make_async_copy(staged.at[r, s], ret.at[item], ret_sem).start()
+                    pltpu.make_async_copy(staged.at[r, s], ret.at[place], ret_sem.at[group]).start()
 
                 @pl.when(me != s)
                 def _():
                     pltpu.make_async_remote_copy(
                         src_ref=staged.at[r, s],
-                        dst_ref=ret.at[item],
+                        dst_ref=ret.at[place],
                         send_sem=back_sem,
-                        recv_sem=ret_sem,
+                        recv_sem=ret_sem.at[group],
                         device_id={"sp": s},
                     ).start()
 
@@ -320,22 +356,6 @@
         @pl.when((is_low & (kind == 0)) | is_high)
         def _():
             part(half, half)
-
-        @pl.when((r == rows // 16) & is_gate)
-        def _():
-            w_far(True)
-
-        @pl.when((r == rows // 4) & jnp.logical_not(is_gate))
-        def _():
-            w_far(False)
-
-        @pl.when(r == rows // 2)
-        def _():
-            w_side()
-
-        @pl.when(r == rows - rows // 4)
-        def _():
-            w_across()
 
         return carry
 
@@ -364,20 +384,34 @@
     drain(recv.at[0, pl.ds(0, 2)], send_sem, jnp.where(low, doubles, 0))
     drain(w_at(me, col), w_send_sem, w_sends)
 
-    gate_copy.wait()
-    pltpu.make_async_copy(ret, ret, ret_sem).wait()
-    for s in range(seqs):
-        for h in range(heads):
-            logits = gate_v[:, s, h * cols : (h + 1) * cols].astype(jnp.float32)
-            gated[s * toks : (s + 1) * toks, h * cols : (h + 1) * cols] = (
-                jax.nn.sigmoid(logits) * ret[s * heads + h].astype(jnp.float32)
-            ).astype(jnp.bfloat16)
+    per_group = items // GROUPS
+
+    def gate_group(g):
+        part = ret.at[pl.ds(g * per_group, per_group)]
+        arrived(part, ret_sem.at[g])
+        for place in range(g * per_group, (g + 1) * per_group):
+            h, s = place // seqs, place % seqs
+            at = (h, pl.ds(s, toks, stride=seqs))
+            gated[at] = gated[at] * ret[place].astype(jnp.float32)
+
+    def gated_rows(first, end):
+        return jnp.concatenate([gated[h].astype(jnp.bfloat16) for h in range(first, end)], axis=1)
+
+    last_head = heads - heads // GROUPS
+    last = last_head * cols
+    for g in range(GROUPS - 1):
+        gate_group(g)
     for d in range(m):
-        result = jnp.dot(gated[...], wbuf[d], preferred_element_type=jnp.float32)
-        for s in range(seqs):
-            out_ref[s, :, d * w_cols : (d + 1) * w_cols] = result[s * toks : (s + 1) * toks].astype(
-                jnp.bfloat16
-            )
+        partial[:, d * w_cols : (d + 1) * w_cols] = jnp.dot(
+            gated_rows(0, last_head), wbuf[d, :last], preferred_element_type=jnp.float32
+        )
+    gate_group(GROUPS - 1)
+    for d in range(m):
+        at = slice(d * w_cols, (d + 1) * w_cols)
+        result = partial[:, at] + jnp.dot(
+            gated_rows(last_head, heads), wbuf[d, last:], preferred_element_type=jnp.float32
+        )
+        out_ref[:, :, at] = result.astype(jnp.bfloat16).reshape(toks, seqs, w_cols)
     drain(staged.at[0, 0], back_sem, backs)
 
 
@@ -391,7 +425,7 @@
     in_vmem = pl.BlockSpec(memory_space=pltpu.VMEM)
     result = pl.pallas_call(
         functools.partial(layer_kernel, n, m, heads),
-        out_shape=jax.ShapeDtypeStruct((seqs, toks, width), jnp.bfloat16),
+        out_shape=jax.ShapeDtypeStruct((toks, seqs, width), jnp.bfloat16),
         in_specs=[
             anywhere, anywhere, anywhere, anywhere, pl.BlockSpec(memory_space=pltpu.SMEM), in_vmem, anywhere,
         ],
@@ -402,17 +436,18 @@
             pltpu.VMEM((items, toks, cols), jnp.bfloat16),
             pltpu.VMEM((m, n * w_rows, w_cols), jnp.bfloat16),
             pltpu.VMEM(gate_logits.shape, jnp.bfloat16),
-            pltpu.VMEM((seqs * toks, width), jnp.bfloat16),
+            pltpu.VMEM((heads, toks * seqs, cols), jnp.float32),
+            pltpu.VMEM((toks * seqs, width), jnp.float32),
             pltpu.SemaphoreType.DMA((rows,)),
             pltpu.SemaphoreType.DMA,
-            pltpu.SemaphoreType.DMA,
+            pltpu.SemaphoreType.DMA((GROUPS,)),
             pltpu.SemaphoreType.DMA,
             pltpu.SemaphoreType.DMA((n, m)),
             pltpu.SemaphoreType.DMA,
             pltpu.SemaphoreType.DMA,
         ],
         compiler_params=pltpu.CompilerParams(
-            collective_id=0, has_side_effects=True, vmem_limit_bytes=60 * 2**20
+            collective_id=0, has_side_effects=True, vmem_limit_bytes=52 * 2**20
         ),
         cost_estimate=pl.CostEstimate(flops=5 * 10**10, bytes_accessed=2**28, transcendentals=0),
     )(
@@ -424,7 +459,7 @@
         head_gain.reshape(1, cols),
         out_weight,
     )
-    return jnp.transpose(result, (1, 0, 2))
+    return result
 
 
 def solution(mesh):

time: 117 us -> 96.3 us (0.82)
  Pallas kernels: 114 us -> 93.5 us
    pallas_call x1, Pallas kernels: 114 us -> 93.5 us  [on_device(): pl.pallas_call(functools.partial(layer_kernel, n, m, heads), out_shape=ja...]
    transpose x1 -> x0, local copies, waits for them, and re-layouts: 3.01 us -> none  [on_device(): return jnp.transpose(result, (1, 0, 2))]
    unnamed x0 -> x7, local copies, waits for them, and re-layouts: none -> 2.59 us
where the time goes in v2:
time: 96.3 us; the launch traced here: 96.1 us
  Pallas kernels  93.5 us (97%)
  local copies, waits for them, and re-layouts  2.59 us (3%)
    pallas_call x1, Pallas kernels, on_device(): pl.pallas_call(functools.partial(layer_kernel, n, m, heads), out_shape=ja...  93.5 us
    unnamed x7, local copies, waits for them, and re-layouts  2.59 us

profile of v2, /device:TPU:0, one launch (start us, length us, event | category | flops | bytes accessed | tf_op | source)
XLA Modules:
  0.0 96.1 jit_solution(8407093607389563263)
XLA Ops:
  0.0 0.0 copy-start.1
  0.0 0.0 copy-start.2
  0.0 0.7 copy-done.1
  0.7 0.0 copy-done.2
  0.7 0.0 copy-start
  0.7 0.9 copy-done
  1.6 93.5 %shard_map.73 = bf16[64,4,2048]{2,1,0:T(4,128)(2,1)S(1)} custom-call(bf16[64,64,128]{2,1,0:T(8,128)(2,1)} %bitcast.5, bf16[64,64,128]{2,1,0:T(8,128)(2,1)} %bitcast.6, bf16[64,64,128]{2,1,0:T(8,128)(2,1)} %bitcast.7, bf16[64,4,2048]{2,1,0:T(4,128)(2,1)} %gate_ref.1, f32[16]{0:T(128)S(1)} %copy-done.1, f32[1,128]{1,0:T(1,128)S(1)} %bitcast.4, ...), custom_call_target="tpu_custom_call" | custom-call | flops 49999998976 | bytes 268435456 | tf_op jit(solution)/shard_map/pallas_call | solution.py:426
  95.1 1.0 %copy.9 = bf16[64,4,2048]{2,1,0:T(4,128)(2,1)} copy(bf16[64,4,2048]{2,1,0:T(4,128)(2,1)S(1)} %shard_map.73) | data formatting | bytes 2097152
Async XLA Ops:
  0.0 0.7 copy-start.1
  0.0 0.7 copy-start.2
  0.7 0.9 copy-start

commit v3 on v2

--- a/solution.py
+++ b/solution.py
@@ -10,7 +10,7 @@
 HEAD_DIM = 64
 STRETCH = 64
 LOG2E = 1.4426950408889634
-GROUPS = 8
+GROUPS = 4
 WINDOW = 16
 NEAR = 0
 GATE = 1
@@ -46,6 +46,17 @@
 
 def item_at(place, seqs, heads):
     return lax.rem(place, seqs) * heads + place // seqs
+
+
+def grid_of(n):
+    ys = 1
+    while 2 * (2 * ys) ** 2 <= n:
+        ys *= 2
+    return ys, n // ys
+
+
+def rounds_of(zs, ys):
+    return max(zs - 1 + (ys > 1) - 1, 1)
 
 
 def pick(table, index):
@@ -88,7 +99,7 @@
 def layer_kernel(
     n, m, heads, q_ref, k_ref, v_ref, gate_ref, lam_ref, gain_ref, w_ref, out_ref,
     recv, staged, ret, wbuf, gate_v, gated, partial,
-    recv_sem, send_sem, ret_sem, back_sem, w_sem, w_send_sem, gate_sem,
+    recv_sem, send_sem, ret_sem, back_sem, w_sem, w_send_sem, gate_sem, round_sem,
 ):
     me = lax.axis_index("sp")
     col = lax.axis_index("dp")
@@ -105,19 +116,26 @@
 
     cores = 2 if m % 2 == 0 else 1
     xs = m // cores
-    ys = 1
-    while 2 * (2 * ys) ** 2 <= n:
-        ys *= 2
-    zs = n // ys
+    ys, zs = grid_of(n)
     hz = zs // 2
     my_z, my_y = me // ys, lax.rem(me, ys)
     my_x, my_core = col // cores, lax.rem(col, cores)
 
     barrier = pltpu.get_barrier_semaphore()
 
-    def greet_sp(step, carry):
-        pl.semaphore_signal(barrier, inc=1, device_id={"sp": lax.rem(me + step, n)})
-        return carry
+    def greet_near(sem):
+        @pl.when(my_z > 0)
+        def _():
+            pl.semaphore_signal(sem, inc=1, device_id={"sp": me - ys})
+
+        @pl.when(my_z < zs - 1)
+        def _():
+            pl.semaphore_signal(sem, inc=1, device_id={"sp": me + ys})
+
+        for i in range(1, ys):
+            pl.semaphore_signal(sem, inc=1, device_id={"sp": my_z * ys + lax.rem(my_y + i, ys)})
+
+    near_count = jnp.where(my_z > 0, 1, 0) + jnp.where(my_z < zs - 1, 1, 0) + ys - 1
 
     def greet_dp(step, carry):
         pl.semaphore_signal(barrier, inc=1, device_id={"dp": lax.rem(col + step, m)})
@@ -125,14 +143,14 @@
 
     gate_copy = pltpu.make_async_copy(gate_ref, gate_v, gate_sem)
     gate_copy.start()
-    lax.fori_loop(1, n, greet_sp, 0)
+    greet_near(barrier)
     lax.fori_loop(1, m, greet_dp, 0)
 
     def w_at(s, d):
         return wbuf.at[d, pl.ds(pl.multiple_of(s * w_rows, w_rows), w_rows)]
 
     pltpu.make_async_copy(w_ref, w_at(me, col), w_sem.at[me, col]).start()
-    pl.semaphore_wait(barrier, n - 1 + m - 1)
+    pl.semaphore_wait(barrier, near_count + m - 1)
 
     def w_send(src, s, d, **target):
         pltpu.make_async_remote_copy(
@@ -163,11 +181,23 @@
     far_z = hz - base_z
     is_gate = my_z == jnp.where(low, hz - 1, hz)
 
-    w_send(w_ref, me, col, sp=jnp.where(low, hz, hz - 1) * ys + my_y)
-    to_half_peers(w_ref, me, col)
+    def to_gate():
+        w_send(w_ref, me, col, sp=jnp.where(low, hz, hz - 1) * ys + my_y)
+
+    greet_near(round_sem.at[0])
+    pl.when(is_gate)(to_gate)
     to_ys(w_ref, me, col)
+    if hz == 2:
+        to_half_peers(w_ref, me, col)
     to_xs(w_ref, me, col)
     to_core(w_ref, me, col)
+    pl.semaphore_wait(round_sem.at[0], near_count)
+    for i in range(1, rounds_of(zs, ys)):
+        greet_near(round_sem.at[i])
+        pl.semaphore_wait(round_sem.at[i], near_count)
+    pl.when(jnp.logical_not(is_gate))(to_gate)
+    if hz != 2:
+        to_half_peers(w_ref, me, col)
 
     def w_near():
         for i in range(1, ys):
@@ -316,13 +346,7 @@
             k = recv[r, n : n + first + count].reshape((first + count) * toks, cols)
             v = recv[r, 2 * n : 2 * n + first + count].reshape((first + count) * toks, cols)
 
-            def store(at, block):
-                for i in range(0, block.shape[0], toks):
-                    staged[r, first + (at + i) // toks] = block[i : i + toks]
-
-            attend(q, k, v, first * toks, weight_two, gain, store)
-            for s in range(first, first + count):
-
+            def give_back(s):
                 @pl.when(me == s)
                 def _():
                     pltpu.make_async_copy(staged.at[r, s], ret.at[place], ret_sem.at[group]).start()
@@ -336,6 +360,14 @@
                         recv_sem=ret_sem.at[group],
                         device_id={"sp": s},
                     ).start()
+
+            def store(at, block):
+                for i in range(0, block.shape[0], toks):
+                    staged[r, first + (at + i) // toks] = block[i : i + toks]
+                for i in range(0, block.shape[0], toks):
+                    give_back(first + (at + i) // toks)
+
+            attend(q, k, v, first * toks, weight_two, gain, store)
 
         @pl.when(is_low & (kind == 0))
         def _():
@@ -421,6 +453,7 @@
     rows = items // (n // 4)
     width = gate_logits.shape[2]
     w_rows, w_cols = out_weight.shape
+    ys, zs = grid_of(n)
     anywhere = pl.BlockSpec(memory_space=pl.ANY)
     in_vmem = pl.BlockSpec(memory_space=pltpu.VMEM)
     result = pl.pallas_call(
@@ -445,6 +478,7 @@
             pltpu.SemaphoreType.DMA((n, m)),
             pltpu.SemaphoreType.DMA,
             pltpu.SemaphoreType.DMA,
+            pltpu.SemaphoreType.REGULAR((rounds_of(zs, ys),)),
         ],
         compiler_params=pltpu.CompilerParams(
             collective_id=0, has_side_effects=True, vmem_limit_bytes=52 * 2**20

time: 96.3 us -> 94.5 us (0.981)
  Pallas kernels: 93.5 us -> 91.7 us
    pallas_call x1, Pallas kernels: 93.5 us -> 91.7 us  [on_device(): pl.pallas_call(functools.partial(layer_kernel, n, m, heads), out_shape=ja...]
where the time goes in v3:
time: 94.5 us; the launch traced here: 94.3 us
  Pallas kernels  91.7 us (97%)
  local copies, waits for them, and re-layouts  2.59 us (3%)
    pallas_call x1, Pallas kernels, on_device(): pl.pallas_call(functools.partial(layer_kernel, n, m, heads), out_shape=ja...  91.7 us
    unnamed x7, local copies, waits for them, and re-layouts  2.59 us

profile of v3, /device:TPU:0, one launch (start us, length us, event | category | flops | bytes accessed | tf_op | source)
XLA Modules:
  0.0 94.3 jit_solution(2599757861746442074)
XLA Ops:
  0.0 0.0 copy-start.1
  0.0 0.0 copy-start.2
  0.0 0.7 copy-done.1
  0.7 0.0 copy-done.2
  0.7 0.0 copy-start
  0.7 0.9 %copy-done = bf16[256,512]{1,0:T(8,128)(2,1)S(1)} copy-done((bf16[256,512]{1,0:T(8,128)(2,1)S(1)}, bf16[256,512]{1,0:T(8,128)(2,1)}, u32[]{:S(2)}) %copy-start) | copy-done | bytes 262168
  1.6 91.7 %shard_map.73 = bf16[64,4,2048]{2,1,0:T(4,128)(2,1)S(1)} custom-call(bf16[64,64,128]{2,1,0:T(8,128)(2,1)} %bitcast.5, bf16[64,64,128]{2,1,0:T(8,128)(2,1)} %bitcast.6, bf16[64,64,128]{2,1,0:T(8,128)(2,1)} %bitcast.7, bf16[64,4,2048]{2,1,0:T(4,128)(2,1)} %gate_ref.1, f32[16]{0:T(128)S(1)} %copy-done.1, f32[1,128]{1,0:T(1,128)S(1)} %bitcast.4, ...), custom_call_target="tpu_custom_call" | custom-call | flops 49999998976 | bytes 268435456 | tf_op jit(solution)/shard_map/pallas_call | solution.py:459
  93.4 1.0 %copy.9 = bf16[64,4,2048]{2,1,0:T(4,128)(2,1)} copy(bf16[64,4,2048]{2,1,0:T(4,128)(2,1)S(1)} %shard_map.73) | data formatting | bytes 2097152
Async XLA Ops:
  0.0 0.7 copy-start.1
  0.0 0.7 copy-start.2
  0.7 0.9 %copy-start = (bf16[256,512]{1,0:T(8,128)(2,1)S(1)}, bf16[256,512]{1,0:T(8,128)(2,1)}, u32[]{:S(2)}) copy-start(bf16[256,512]{1,0:T(8,128)(2,1)} %w_ref.1) | copy-start | bytes 786436

commit v4 on v3

--- a/solution.py
+++ b/solution.py
@@ -13,8 +13,9 @@
 GROUPS = 4
 WINDOW = 16
 NEAR = 0
-GATE = 1
+GATE = 0
 FAR = 9
+BESIDE = 13
 SIDE = 17
 ACROSS = 25
 
@@ -222,10 +223,11 @@
             to_xs(w_at(s, col), s, col)
             to_core(w_at(s, col), s, col)
 
-    def w_side():
+    def w_side(own_half):
         for j in range(1, ys):
-            for i in range(1, zs):
-                s = lax.rem(my_z + i, zs) * ys + lax.rem(my_y + j, ys)
+            for i in range(1 if own_half else 0, hz):
+                z = base_z + lax.rem(my_z - base_z + i, hz) if own_half else far_z + i
+                s = z * ys + lax.rem(my_y + j, ys)
                 w_wait(s, col)
                 to_xs(w_at(s, col), s, col)
                 to_core(w_at(s, col), s, col)
@@ -260,7 +262,8 @@
     def send_row(r):
         kind, low_q, high_q = pick(kinds, r), pick(lows, r), pick(highs, r)
 
-        def send_item(c, carry):
+        def send_item(step, carry):
+            c = lax.rem(step + my_column, quarter)
             item = item_at(r * quarter + c, seqs, heads)
             first = jnp.where((kind == 0) | low, low_q, high_q) * quarter + c
 
@@ -325,9 +328,13 @@
         def _():
             w_far(False)
 
+        @pl.when(r == BESIDE * rows // 32)
+        def _():
+            w_side(True)
+
         @pl.when(r == SIDE * rows // 32)
         def _():
-            w_side()
+            w_side(False)
 
         @pl.when(r == ACROSS * rows // 32)
         def _():

time: 94.5 us -> 94.3 us (level)
  no operation moved by 1% of the time
where the time goes in v4:
time: 94.3 us; the launch traced here: 94.2 us
  Pallas kernels  91.6 us (97%)
  local copies, waits for them, and re-layouts  2.59 us (3%)
    pallas_call x1, Pallas kernels, on_device(): pl.pallas_call(functools.partial(layer_kernel, n, m, heads), out_shape=ja...  91.6 us
    unnamed x7, local copies, waits for them, and re-layouts  2.59 us

profile of v4, /device:TPU:0, one launch (start us, length us, event | category | flops | bytes accessed | tf_op | source)
XLA Modules:
  0.0 94.2 jit_solution(13641214936893334389)
XLA Ops:
  0.0 0.0 copy-start.1
  0.0 0.0 copy-start.2
  0.0 0.7 copy-done.1
  0.7 0.0 copy-done.2
  0.7 0.0 copy-start
  0.7 0.9 %copy-done = bf16[256,512]{1,0:T(8,128)(2,1)S(1)} copy-done((bf16[256,512]{1,0:T(8,128)(2,1)S(1)}, bf16[256,512]{1,0:T(8,128)(2,1)}, u32[]{:S(2)}) %copy-start) | copy-done | bytes 262168
  1.6 91.6 %shard_map.73 = bf16[64,4,2048]{2,1,0:T(4,128)(2,1)S(1)} custom-call(bf16[64,64,128]{2,1,0:T(8,128)(2,1)} %bitcast.5, bf16[64,64,128]{2,1,0:T(8,128)(2,1)} %bitcast.6, bf16[64,64,128]{2,1,0:T(8,128)(2,1)} %bitcast.7, bf16[64,4,2048]{2,1,0:T(4,128)(2,1)} %gate_ref.1, f32[16]{0:T(128)S(1)} %copy-done.1, f32[1,128]{1,0:T(1,128)S(1)} %bitcast.4, ...), custom_call_target="tpu_custom_call" | custom-call | flops 49999998976 | bytes 268435456 | tf_op jit(solution)/shard_map/pallas_call | solution.py:466
  93.2 1.0 %copy.9 = bf16[64,4,2048]{2,1,0:T(4,128)(2,1)} copy(bf16[64,4,2048]{2,1,0:T(4,128)(2,1)S(1)} %shard_map.73) | data formatting | bytes 2097152
Async XLA Ops:
  0.0 0.7 copy-start.1
  0.0 0.7 copy-start.2
  0.7 0.9 %copy-start = (bf16[256,512]{1,0:T(8,128)(2,1)S(1)}, bf16[256,512]{1,0:T(8,128)(2,1)}, u32[]{:S(2)}) copy-start(bf16[256,512]{1,0:T(8,128)(2,1)} %w_ref.1) | copy-start | bytes 786436
